TPU v7x, 32 devices: a whole 2x2x4 slice. The times are simulated.
32 devices in a mesh: kv: 4 (over y, x), tp: 8 (over z, core).
Axes of the slice: x: 2, y: 2, z: 4, core: 2. Of those that a mesh axis runs over, the one named last changes fastest.
Arguments:
- tokens: bfloat16 [128, 4096], P(None, 'tp'), may hold values from -6 to 6
- norm_gain: float32 [4096], P('tp'), may hold values from 0.1 to 1.9
- query_weight: bfloat16 [4096, 2048], P('tp', 'kv'), may hold values from -0.09375 to 0.09375
- key_weight: bfloat16 [4096, 2048], P('tp', 'kv'), may hold values from -0.09375 to 0.09375
- value_weight: bfloat16 [4096, 2048], P('tp', 'kv'), may hold values from -0.09375 to 0.09375
- input_gate_weight: bfloat16 [4096, 16], P('tp'), may hold values from -0.09375 to 0.09375
- forget_gate_weight: bfloat16 [4096, 16], P('tp'), may hold values from -0.09375 to 0.09375
- input_gate_bias: float32 [16], P('kv'), may hold values from -2 to 2
- forget_gate_bias: float32 [16], P('kv'), may hold values from 1 to 6
- memory_state: float32 [128, 16, 128, 128], P('tp', 'kv'), may hold values from -12 to 12
- normalizer_state: float32 [128, 16, 128], P('tp', 'kv'), may hold values from -24 to 24
- stabilizer_state: float32 [128, 16], P('tp', 'kv'), may hold values from -1 to 3
- block_keys: bfloat16 [128, 16, 128, 128], P('tp', 'kv'), may hold values from -6 to 6
- block_values: bfloat16 [128, 16, 128, 128], P('tp', 'kv'), may hold values from -6 to 6
- block_input_pre: float32 [128, 16, 128], P('tp', 'kv'), may hold values from -6 to 6
- block_forget_pre: float32 [128, 16, 128], P('tp', 'kv'), may hold values from -6 to 6
- block_lengths: int32 [128], P('tp'), may hold values from 1 to 128, 6553 in all
- head_norm_gain: float32 [2048], P('kv'), may hold values from 0.1 to 1.9
- output_weight: bfloat16 [2048, 4096], P('kv', 'tp'), may hold values from -0.125 to 0.125
- mixer_norm_gain: float32 [4096], P('tp'), may hold values from 0.1 to 1.9
- gate_weight: bfloat16 [4096, 11264], P('tp', 'kv'), may hold values from -0.09375 to 0.09375
- up_weight: bfloat16 [4096, 11264], P('tp', 'kv'), may hold values from -0.09375 to 0.09375
- down_weight: bfloat16 [11264, 4096], P('kv', 'tp'), may hold values from -0.0546875 to 0.0546875
Outputs:
- layer_output: float32 [128, 4096], P(None, 'tp')
Inputs may be any that keep to these rules, and one draw needn't show every extreme that they name: `block_lengths`: some sequence has exactly 128 live positions.
All inputs are finite; a program needn't handle non-finite values. No bound on the sum of `block_lengths` on one device may be relied on, other than what follows from the above.
Results may differ from a plain program's by a relative error of at most 0.0078.
Values may be sent and summed in bfloat16 or wider, within the bound.
A program may use at most 64 MiB of HBM per device.

v0:
```python
import jax
import jax.numpy as jnp
from jax import lax
from jax.sharding import PartitionSpec as P

D = 4096


epsilon = 1e-06


def memory_cell(
    queries,
    new_keys,
    new_values,
    log_input,
    log_forget,
    memory,
    normalizer,
    stabilizer,
    cached_keys,
    cached_values,
    input_pre,
    forget_pre,
    lengths,
    input_bias,
    forget_bias,
):
    positions = jnp.arange(cached_keys.shape[2])
    is_live = (positions[None, :] < lengths[:, None])[:, None, :]
    cached_input = input_pre + input_bias[None, :, None]
    cached_forget = jnp.where(
        is_live, jax.nn.log_sigmoid(forget_pre + forget_bias[None, :, None]), 0.0
    )
    after_mask = (positions[:, None] > positions[None, :]).astype(jnp.float32)
    later_forget = (
        jnp.einsum("bhu,us->bhs", cached_forget, after_mask, precision=lax.Precision.HIGHEST)
        + log_forget[..., None]
    )
    total_forget = jnp.sum(cached_forget, axis=-1) + log_forget
    exponent = jnp.where(is_live, later_forget + cached_input, -jnp.inf)
    carried = total_forget + stabilizer
    stab_max = jnp.maximum(jnp.maximum(jnp.max(exponent, axis=-1), carried), log_input)
    scores = jnp.einsum("bhd,bhsd->bhs", queries, cached_keys, preferred_element_type=jnp.float32)
    block_weight = jnp.exp(exponent - stab_max[..., None]) * scores
    block_probs = block_weight.astype(jnp.bfloat16)
    block_sum = jnp.einsum(
        "bhs,bhsd->bhd", block_probs, cached_values, preferred_element_type=jnp.float32
    )
    query_wide = queries.astype(jnp.float32)
    new_weight = jnp.exp(log_input - stab_max) * jnp.sum(
        query_wide * new_keys.astype(jnp.float32), axis=-1
    )
    state_weight = jnp.exp(carried - stab_max)
    state_sum = jnp.einsum("bhkv,bhk->bhv", memory, query_wide, precision=lax.Precision.HIGHEST)
    state_norm = jnp.sum(normalizer * query_wide, axis=-1)
    numerator = (
        block_sum
        + new_weight[..., None] * new_values.astype(jnp.float32)
        + state_weight[..., None] * state_sum
    )
    denominator = jnp.sum(block_weight, axis=-1) + new_weight + state_weight * state_norm
    return numerator / jnp.maximum(jnp.abs(denominator), 1.0)[..., None]


def head_scale(cell_out, gain):
    return (cell_out * gain.reshape(cell_out.shape[1], cell_out.shape[2])).astype(jnp.bfloat16)


def activate(gate_sum, up_sum, square_sum):
    row_scale = lax.rsqrt(square_sum / D + epsilon)[:, None]
    return (jax.nn.silu(gate_sum * row_scale) * (up_sum * row_scale)).astype(jnp.bfloat16)


def body(
    tokens,
    norm_gain,
    query_weight,
    key_weight,
    value_weight,
    input_gate_weight,
    forget_gate_weight,
    input_gate_bias,
    forget_gate_bias,
    memory_state,
    normalizer_state,
    stabilizer_state,
    block_keys,
    block_values,
    block_input_pre,
    block_forget_pre,
    block_lengths,
    head_norm_gain,
    output_weight,
    mixer_norm_gain,
    gate_weight,
    up_weight,
    down_weight,
):
    seq_rows = block_keys.shape[0]
    heads_dev = block_keys.shape[1]
    head_size = block_keys.shape[3]
    tok_wide = tokens.astype(jnp.float32)
    scaled_in = (tok_wide * norm_gain).astype(jnp.bfloat16)
    square_part = jnp.sum(tok_wide * tok_wide, axis=1)

    def partial_of(weight):
        return jnp.dot(scaled_in, weight, preferred_element_type=jnp.float32)

    query_sum, key_sum, value_sum, input_sum, forget_sum, square_sum = (
        lax.psum_scatter(partial_of(query_weight), "tp", scatter_dimension=0, tiled=True),
        lax.psum_scatter(partial_of(key_weight), "tp", scatter_dimension=0, tiled=True),
        lax.psum_scatter(partial_of(value_weight), "tp", scatter_dimension=0, tiled=True),
        lax.psum_scatter(partial_of(input_gate_weight), "tp", scatter_dimension=0, tiled=True),
        lax.psum_scatter(partial_of(forget_gate_weight), "tp", scatter_dimension=0, tiled=True),
        lax.psum_scatter(square_part, "tp", scatter_dimension=0, tiled=True),
    )
    first_scale = lax.rsqrt(square_sum / D + epsilon)[:, None]
    queries = (
        (query_sum * first_scale * head_size ** (-0.5))
        .astype(jnp.bfloat16)
        .reshape(seq_rows, heads_dev, head_size)
    )
    new_keys = (key_sum * first_scale).astype(jnp.bfloat16).reshape(seq_rows, heads_dev, head_size)
    new_values = (
        (value_sum * first_scale).astype(jnp.bfloat16).reshape(seq_rows, heads_dev, head_size)
    )
    head_start = lax.axis_index("kv") * heads_dev
    log_input = (
        lax.dynamic_slice_in_dim(input_sum * first_scale, head_start, heads_dev, 1)
        + input_gate_bias
    )
    log_forget = jax.nn.log_sigmoid(
        lax.dynamic_slice_in_dim(forget_sum * first_scale, head_start, heads_dev, 1)
        + forget_gate_bias
    )
    cell_out = memory_cell(
        queries,
        new_keys,
        new_values,
        log_input,
        log_forget,
        memory_state,
        normalizer_state,
        stabilizer_state,
        block_keys,
        block_values,
        block_input_pre,
        block_forget_pre,
        block_lengths,
        input_gate_bias,
        forget_gate_bias,
    )
    head_out = head_scale(cell_out, head_norm_gain).reshape(seq_rows, heads_dev * head_size)
    attended_part = jnp.dot(
        lax.all_gather(head_out, "tp", axis=0, tiled=True),
        output_weight,
        preferred_element_type=jnp.float32,
    )
    attended = lax.psum(attended_part, "kv")
    res_wide = tok_wide + attended
    mid_square = jnp.sum(res_wide * res_wide, axis=1)
    mid_scaled = (res_wide * mixer_norm_gain).astype(jnp.bfloat16)
    gate_part = jnp.dot(mid_scaled, gate_weight, preferred_element_type=jnp.float32)
    up_part = jnp.dot(mid_scaled, up_weight, preferred_element_type=jnp.float32)
    gate_sum, up_sum, mid_sum = lax.psum((gate_part, up_part, mid_square), "tp")
    hidden = activate(gate_sum, up_sum, mid_sum)
    down_part = jnp.dot(hidden, down_weight, preferred_element_type=jnp.float32)
    mixed = lax.psum(down_part, "kv")
    return res_wide + mixed


def solution(mesh):
    placed = (
        P(None, "tp"),
        P("tp"),
        P("tp", "kv"),
        P("tp", "kv"),
        P("tp", "kv"),
        P("tp", None),
        P("tp", None),
        P("kv"),
        P("kv"),
        P("tp", "kv", None, None),
        P("tp", "kv", None),
        P("tp", "kv"),
        P("tp", "kv", None, None),
        P("tp", "kv", None, None),
        P("tp", "kv", None),
        P("tp", "kv", None),
        P("tp"),
        P("kv"),
        P("kv", "tp"),
        P("tp"),
        P("tp", "kv"),
        P("tp", "kv"),
        P("kv", "tp"),
    )
    return jax.shard_map(body, mesh=mesh, in_specs=placed, out_specs=P(None, "tp"), check_vma=False)
```

profile of v0, /device:TPU:0, one launch (start us, length us, event | category | flops | bytes accessed | tf_op | source)
XLA Modules:
  0.0 376.3 jit_solution(17206025061885807073)
XLA Ops:
  6.5 0.0 reduce-scatter.16.cloned.1.call-start
  6.6 1.9 fusion.16
  8.5 0.0 reduce-scatter.16.cloned.1.call-update
  8.5 0.0 reduce-scatter.18.cloned.1.call-start
  8.5 1.7 fusion.14
  10.2 0.0 reduce-scatter.18.cloned.1.call-update
  10.3 0.0 reduce-scatter.10.cloned.1.call-start
  10.3 2.1 fusion.12
  12.4 0.0 reduce-scatter.10.cloned.1.call-update
  12.4 0.0 reduce-scatter.12.cloned.1.call-start
  12.5 2.1 fusion.10
  14.5 0.0 reduce-scatter.12.cloned.1.call-update
  14.6 0.0 reduce-scatter.14.cloned.1.call-start
  14.6 0.9 fusion.8
  15.6 0.0 reduce-scatter.14.cloned.1.call-update
  15.6 0.0 all-reduce.6.cloned.1.call-start
  15.7 0.1 fusion.4
  15.8 18.1 %all-reduce = f32[128]{0:T(128)S(1)} all-reduce(f32[128]{0:T(128)S(1)} %fusion.4), channel_id=3, replica_groups=mesh['kv'=4,'tp'=8] {'tp'}, use_global_device_ids=true, to_apply=%region_2.0.clone | all-reduce | flops 128 | bytes 1024
  33.9 0.7 iota_compare_fusion.1
  34.6 1.3 dynamic-slice
  36.6 0.1 fusion.30
  36.7 0.9 fusion.32
  37.7 5.3 %reduce-scatter.16.cloned.1.call-done = f32[16,16]{1,0:T(8,128)} async-done(((f32[128,16]{1,0:T(8,128)}), f32[16,16]{1,0:T(8,128)}) %reduce-scatter.16.cloned.1.call-update) | async-done | bytes 1040
  42.9 0.8 constant_dynamic-slice_fusion.1
  43.7 0.1 copy.64
  43.8 0.1 fusion.28
  43.9 29.9 %reduce-scatter.18.cloned.1.call-done = f32[16,16]{1,0:T(8,128)} async-done(((f32[128,16]{1,0:T(8,128)}), f32[16,16]{1,0:T(8,128)}) %reduce-scatter.18.cloned.1.call-update) | async-done | bytes 1040
  73.8 0.8 constant_dynamic-slice_fusion
  74.5 0.1 copy.65
  74.6 1.6 fusion.34
  76.3 0.7 maximum_maximum_fusion
  76.9 27.9 %reduce-scatter.10.cloned.1.call-done = f32[16,512]{1,0:T(8,128)} async-done(((f32[128,512]{1,0:T(8,128)}), f32[16,512]{1,0:T(8,128)}) %reduce-scatter.10.cloned.1.call-update) | async-done | bytes 32784 | tf_op jit(solution)/shard_map/reduce_scatter | solution.py:111
  104.9 31.1 %reduce-scatter.12.cloned.1.call-done = f32[16,512]{1,0:T(8,128)} async-done(((f32[128,512]{1,0:T(8,128)}), f32[16,512]{1,0:T(8,128)}) %reduce-scatter.12.cloned.1.call-update) | async-done | bytes 32784 | tf_op jit(solution)/shard_map/reduce_scatter | solution.py:112
  136.0 31.1 %reduce-scatter.14.cloned.1.call-done = f32[16,512]{1,0:T(8,128)} async-done(((f32[128,512]{1,0:T(8,128)}), f32[16,512]{1,0:T(8,128)}) %reduce-scatter.14.cloned.1.call-update) | async-done | bytes 32784 | tf_op jit(solution)/shard_map/reduce_scatter | solution.py:113
  167.0 1.5 fusion.25
  168.6 0.9 fusion.18
  169.5 0.6 copy.48
  170.1 0.6 copy.51
  170.8 4.9 %fusion.36 = f32[16,4,1,128]{3,2,1,0:T(1,128)} fusion(bf16[16,4,128,1]{2,3,1,0:T(2,128)(2,1)S(1)} %reshape.54, f32[16,4,128,128]{3,2,1,0:T(8,128)} %param.32), kind=kOutput, calls=%fused_computation.61 | convolution fusion | flops 12582912 | bytes 4243456 | tf_op jit(solution)/shard_map/bhkv,bhk->bhv/dot_general | solution.py:55
  175.8 2.0 fusion.35
  177.8 0.2 fusion.27
  178.1 0.7 abs_maximum_fusion
  178.8 1.3 copy.52
  180.1 1.3 copy.49
  181.5 1.3 copy.50
  182.8 1.4 reshape.46
  184.2 2.3 fusion.22
  186.6 0.1 multiply_convert_fusion.3
  186.7 14.0 %all_gather.3 = bf16[128,512]{1,0:T(8,128)(2,1)S(1)} all-gather(bf16[16,512]{1,0:T(8,128)(2,1)S(1)} %bitcast.45), channel_id=1, replica_groups=mesh['kv'=4,'tp'=8] {'tp'}, dimensions={0}, use_global_device_ids=true | all-gather | bytes 147456 | tf_op jit(solution)/shard_map/all_gather | solution.py:156
  200.7 0.9 fusion.37
  201.6 0.0 all-reduce.6.cloned.1.call-update
  201.6 0.0 all-reduce.10.cloned.1.call-start
  201.7 41.3 %all-reduce.6.cloned.1.call-done = f32[128,512]{1,0:T(8,128)} async-done(((f32[128,512]{1,0:T(8,128)}), f32[128,512]{1,0:T(8,128)}) %all-reduce.6.cloned.1.call-update) | async-done | bytes 262160 | tf_op jit(solution)/shard_map/psum | solution.py:160
  243.0 1.1 multiply_reduce_fusion
  244.1 1.7 fusion.39
  245.7 0.7 copy-done.2
  246.4 1.7 fusion.38
  248.1 0.0 all-reduce.10.cloned.1.call-update
  248.1 0.0 all-reduce.8.cloned.1.call-start
  248.2 16.2 %psum.37 = f32[128]{0:T(128)S(1)} all-reduce(f32[128]{0:T(128)S(1)} %get-tuple-element.12), channel_id=1, replica_groups=mesh['kv'=4,'tp'=8] {'tp'}, use_global_device_ids=true, to_apply=%region_15.16 | all-reduce | flops 128 | bytes 1024 | tf_op jit(solution)/shard_map/psum | solution.py:166
  264.4 56.5 %all-reduce.10.cloned.1.call-done = (f32[128,2816]{1,0:T(8,128)}, f32[128,2816]{1,0:T(8,128)}) async-done(((f32[128,2816]{1,0:T(8,128)}, f32[128,2816]{1,0:T(8,128)}), (f32[128,2816]{1,0:T(8,128)}, f32[128,2816]{1,0:T(8,128)})) %all-reduce.10.cloned.1.call-update) | async-done | bytes 2883600 | tf_op jit(solution)/shard_map/psum | solution.py:166
  320.9 4.2 %fusion.2 = f32[128,512]{1,0:T(8,128)} fusion(bf16[2816,512]{1,0:T(8,128)(2,1)} %param.45, f32[128,2816]{1,0:T(8,128)} %get-tuple-element.7, f32[128,2816]{1,0:T(8,128)} %get-tuple-element.8, f32[128]{0:T(128)S(1)} %add_rsqrt_fusion), kind=kOutput, calls=%fused_computation.4 | convolution fusion | flops 371982336 | bytes 6029824 | tf_op jit(solution)/shard_map/dot_general | solution.py:168
  325.1 42.7 %all-reduce.8.cloned.1.call-done = f32[128,512]{1,0:T(8,128)} async-done(((f32[128,512]{1,0:T(8,128)}), f32[128,512]{1,0:T(8,128)}) %all-reduce.8.cloned.1.call-update) | async-done | bytes 262160 | tf_op jit(solution)/shard_map/psum | solution.py:169
  367.8 1.7 fusion.5
  (71 shorter events, 0.2 us)
Async XLA Ops:
  6.5 237.5 %copy-start = (bf16[512,2816]{1,0:T(8,128)(2,1)S(1)}, bf16[512,2816]{1,0:T(8,128)(2,1)}, u32[]{:S(2)}) copy-start(bf16[512,2816]{1,0:T(8,128)(2,1)} %param.44) | copy-start | bytes 8650756
  6.5 8.1 %copy-start.1 = (bf16[128,512]{1,0:T(8,128)(2,1)S(1)}, bf16[128,512]{1,0:T(8,128)(2,1)}, u32[]{:S(2)}) copy-start(bf16[128,512]{1,0:T(8,128)(2,1)} %param.23) | copy-start | bytes 393220
  6.5 8.1 %copy-start.10 = (f32[512]{0:T(512)S(1)}, f32[512]{0:T(512)}, u32[]{:S(2)}) copy-start(f32[512]{0:T(512)} %param.24) | copy-start | bytes 6148
  6.5 8.1 %copy-start.5 = (bf16[512,512]{1,0:T(8,128)(2,1)S(1)}, bf16[512,512]{1,0:T(8,128)(2,1)}, u32[]{:S(2)}) copy-start(bf16[512,512]{1,0:T(8,128)(2,1)} %param.27) | copy-start | bytes 1572868
  6.5 36.4 %reduce-scatter.16.cloned.1.call-start = ((), (), s32[]{:S(2)}) async-start(), calls=%async_computation.10 | async-start | bytes 73728
  8.5 28.2 %copy-start.22 = (f32[4]{0:T(128)S(1)}, f32[4]{0:T(128)}, u32[]{:S(2)}) copy-start(f32[4]{0:T(128)} %param.31) | copy-start | bytes 52
  8.5 66.2 %copy-start.31 = (f32[4]{0:T(128)S(1)}, f32[4]{0:T(128)}, u32[]{:S(2)}) copy-start(f32[4]{0:T(128)} %param.30) | copy-start | bytes 52
  8.5 65.3 %reduce-scatter.18.cloned.1.call-start = ((), (), s32[]{:S(2)}) async-start(), calls=%async_computation.11 | async-start | bytes 73728
  10.2 66.0 %copy-start.26 = (f32[16,4]{0,1:T(4,128)S(1)}, f32[16,4]{0,1:T(4,128)}, u32[]{:S(2)}) copy-start(f32[16,4]{0,1:T(4,128)} %param.34) | copy-start | bytes 772
  10.3 94.6 %reduce-scatter.10.cloned.1.call-start = ((), (), s32[]{:S(2)}) async-start(), calls=%async_computation.5 | async-start | bytes 294912 | tf_op jit(solution)/shard_map/reduce_scatter | solution.py:111
  12.4 123.5 %reduce-scatter.12.cloned.1.call-start = ((), (), s32[]{:S(2)}) async-start(), calls=%async_computation.6 | async-start | bytes 294912 | tf_op jit(solution)/shard_map/reduce_scatter | solution.py:112
  14.6 152.5 %reduce-scatter.14.cloned.1.call-start = ((), (), s32[]{:S(2)}) async-start(), calls=%async_computation.7 | async-start | bytes 294912 | tf_op jit(solution)/shard_map/reduce_scatter | solution.py:113
  15.6 227.4 %all-reduce.6.cloned.1.call-start = ((), (), s32[]{:S(2)}) async-start(), calls=%async_computation.8 | async-start | bytes 524288 | tf_op jit(solution)/shard_map/psum | solution.py:160
  36.7 131.8 %copy-start.24 = (f32[16]{0:T(128)}, f32[16]{0:T(128)S(1)}, u32[]{:S(2)}) copy-start(f32[16]{0:T(128)S(1)} %fusion.30) | copy-start | bytes 196
  37.6 130.9 %copy-start.17 = (f32[16,4]{0,1:T(4,128)}, f32[16,4]{0,1:T(4,128)S(1)}, u32[]{:S(2)}) copy-start(f32[16,4]{0,1:T(4,128)S(1)} %fusion.32) | copy-start | bytes 772
  43.8 124.7 %copy-start.14 = (f32[16,4]{0,1:T(4,128)}, f32[16,4]{0,1:T(4,128)S(1)}, u32[]{:S(2)}) copy-start(f32[16,4]{0,1:T(4,128)S(1)} %copy.64) | copy-start | bytes 772
  74.6 93.9 %copy-start.19 = (f32[16,4]{0,1:T(4,128)}, f32[16,4]{0,1:T(4,128)S(1)}, u32[]{:S(2)}) copy-start(f32[16,4]{0,1:T(4,128)S(1)} %copy.65) | copy-start | bytes 772
  168.6 2.2 copy-start.7
  170.8 4.9 %copy-start.3 = (bf16[16,4,128,128]{3,2,1,0:T(8,128)(2,1)S(1)}, bf16[16,4,128,128]{3,2,1,0:T(8,128)(2,1)}, u32[]{:S(2)}) copy-start(bf16[16,4,128,128]{3,2,1,0:T(8,128)(2,1)} %param.35) | copy-start | bytes 6291460
  175.7 2.1 copy-start.16
  175.7 2.1 copy-start.21
  175.7 2.3 copy-start.15
  175.7 2.3 copy-start.18
  175.7 2.3 copy-start.20
  175.7 2.3 copy-start.23
  175.8 2.3 copy-start.25
  175.8 2.3 copy-start.27
  175.8 2.3 copy-start.28
  175.8 2.3 copy-start.29
  175.8 2.3 copy-start.32
  175.8 24.9 %copy-start.6 = (bf16[512,512]{1,0:T(8,128)(2,1)S(1)}, bf16[512,512]{1,0:T(8,128)(2,1)}, u32[]{:S(2)}) copy-start(bf16[512,512]{1,0:T(8,128)(2,1)} %param.41) | copy-start | bytes 1572868
  184.2 2.3 copy-start.8
  184.2 2.3 copy-start.9
  184.2 2.3 copy-start.11
  184.2 2.3 copy-start.12
  184.2 2.3 copy-start.13
  184.2 2.3 copy-start.30
  201.6 119.3 %all-reduce.10.cloned.1.call-start = ((), (), s32[]{:S(2)}) async-start(), calls=%async_computation.12 | async-start | bytes 5767168 | tf_op jit(solution)/shard_map/psum | solution.py:166
  244.0 2.3 copy-start.2
  248.1 119.7 %all-reduce.8.cloned.1.call-start = ((), (), s32[]{:S(2)}) async-start(), calls=%async_computation.9 | async-start | bytes 524288 | tf_op jit(solution)/shard_map/psum | solution.py:169
  320.9 46.9 %copy-start.4 = (f32[128,512]{1,0:T(8,128)S(1)}, f32[128,512]{1,0:T(8,128)}, u32[]{:S(2)}) copy-start(f32[128,512]{1,0:T(8,128)} %all-reduce.6.cloned.1.call-done) | copy-start | bytes 786436
Sparse Core Ops, SparseCore 0:
  9.6 33.3 reduce-scatter.15
  45.2 28.5 reduce-scatter.17
  76.0 28.8 reduce-scatter.9
  107.0 28.9 reduce-scatter.11
  138.0 28.9 reduce-scatter.13
  201.8 41.1 all-reduce.5
  248.2 72.6 all-reduce.9
  325.2 42.5 all-reduce.7
where the time goes:
time: 377 us; the launch traced here: 376 us
  waiting for transfers between devices  266 us (71%)
  blocking collectives  48.3 us (13%)
  matrix products  27.9 us (7%)
  between operations  14.5 us (4%)
  local copies, waits for them, and re-layouts  10.6 us (3%)
  other arithmetic  8.77 us (2%)
    psum x1, waiting for transfers between devices, body(): gate_sum, up_sum, mid_sum = lax.psum((gate_part, up_part, mid_square), 'tp')  56.5 us
    psum x1, waiting for transfers between devices, body(): mixed = lax.psum(down_part, 'kv')  42.7 us
    psum x1, waiting for transfers between devices, body(): attended = lax.psum(attended_part, 'kv')  41.3 us
    unnamed x10, waiting for transfers between devices  35.3 us
    reduce_scatter x1, waiting for transfers between devices, body(): lax.psum_scatter(partial_of(key_weight), 'tp', scatter_dimension=0, tiled...  31.1 us
    reduce_scatter x1, waiting for transfers between devices, body(): lax.psum_scatter(partial_of(value_weight), 'tp', scatter_dimension=0, til...  31.1 us
    reduce_scatter x1, waiting for transfers between devices, body(): lax.psum_scatter(partial_of(query_weight), 'tp', scatter_dimension=0, til...  27.9 us
    unnamed x1, blocking collectives  18.1 us
  transfers between devices with their start and end apart: 8, of which 8 were waited for; matrix products, arithmetic and copies ran while one was open for 4% of the time, Pallas kernels for 0%

commit v1 on v0

v1 whole, which is shorter than its diff:
```python
import functools

import jax
import jax.numpy as jnp
from jax import lax
from jax.experimental import pallas as pl
from jax.experimental.pallas import tpu as pltpu
from jax.sharding import PartitionSpec as P

epsilon = 1e-06
MESH = pl.DeviceIdType.MESH
F32, BF16 = jnp.float32, jnp.bfloat16


def log_sigmoid(x):
    return -(jnp.maximum(-x, 0.0) + jnp.log1p(jnp.exp(-jnp.abs(x))))


def dot32(a, b):
    return jnp.dot(a, b, preferred_element_type=F32)


def dot_t(a, b):
    return lax.dot_general(a, b, (((1,), (1,)), ((), ())), preferred_element_type=F32)


class Ring:
    def __init__(self, n_tp, n_kv):
        self.n_tp, self.n_kv, self.nz = n_tp, n_kv, n_tp // 2
        self.t = lax.axis_index("tp")
        self.kv = lax.axis_index("kv")
        self.core = lax.rem(self.t, 2)
        self.z = lax.div(self.t, 2)
        self.partner = self.z * 2 + (1 - self.core)

    def up(self, k):
        return lax.rem(self.z + k, self.nz)

    def down(self, k):
        return lax.rem(self.z + (self.nz - k), self.nz)

    def same(self, z):
        return z * 2 + self.core

    def other(self, z):
        return z * 2 + (1 - self.core)


def remote(src, dst, send, recv, **device):
    return pltpu.make_async_remote_copy(
        src_ref=src, dst_ref=dst, send_sem=send, recv_sem=recv,
        device_id=device, device_id_type=MESH,
    )


class ReduceScatter:
    def __init__(self, ring, sb, rb1, sb2, rb2, sems):
        self.g, self.sb, self.rb1, self.sb2, self.rb2 = ring, sb, rb1, sb2, rb2
        self.s1, self.r1, self.s2, self.r2 = sems

    def pair(self, z):
        g = self.g
        return remote(self.sb.at[g.other(z)], self.rb1.at[z], self.s1.at[z], self.r1.at[z], tp=g.partner)

    def along(self, k):
        g = self.g
        return remote(self.sb2.at[k], self.rb2.at[k], self.s2.at[k], self.r2.at[k], tp=g.same(g.up(k)))

    def order(self):
        return list(range(1, self.g.nz)) + [0]

    def start(self):
        for k in self.order():
            self.pair(self.g.up(k)).start()

    def middle(self):
        g = self.g
        for k in self.order():
            z = g.up(k)
            self.pair(z).wait_recv()
            if k:
                both = self.sb[g.same(z)].astype(F32) + self.rb1[z].astype(F32)
                self.sb2[k] = both.astype(self.sb2.dtype)
                self.along(k).start()

    def end(self):
        g = self.g
        for k in range(1, g.nz):
            self.along(k).wait_recv()
        total = self.sb[g.t].astype(F32) + self.rb1[g.z].astype(F32)
        for k in range(1, g.nz):
            total = total + self.rb2[k].astype(F32)
        return total

    def drain(self):
        for k in range(self.g.nz):
            self.pair(k).wait_send()
        for k in range(1, self.g.nz):
            self.along(k).wait_send()


class Gather:
    def __init__(self, ring, buf, sems):
        self.g, self.buf = ring, buf
        self.s, self.f, self.r = sems

    def direct(self, k):
        g = self.g
        return remote(self.buf.at[g.t], self.buf.at[g.t], self.s.at[k], self.r.at[g.t], tp=g.same(g.up(k)))

    def pass_on(self, block, k):
        g = self.g
        return remote(self.buf.at[block], self.buf.at[block], self.f.at[k], self.r.at[block], tp=g.partner)

    def run(self):
        g = self.g
        for k in range(1, g.nz):
            self.direct(k).start()
        self.pass_on(g.t, 0).start()
        for k in range(1, g.nz):
            copy = self.pass_on(g.same(g.down(k)), k)
            copy.wait_recv()
            copy.start()
        for k in range(g.nz):
            self.pass_on(g.other(g.down(k)), k).wait_recv()

    def drain(self):
        g = self.g
        for k in range(1, g.nz):
            self.direct(k).wait_send()
        for k in range(g.nz):
            self.pass_on(g.same(g.down(k)), k).wait_send()


class SumOverKv:
    def __init__(self, ring, sb, rb, out, sems):
        self.g, self.sb, self.rb, self.out = ring, sb, rb, out
        self.s1, self.r1, self.s2, self.r2 = sems

    def peer(self, k):
        return lax.rem(self.g.kv + k, self.g.n_kv)

    def part(self, k):
        p = self.peer(k)
        return remote(self.sb.at[p], self.rb.at[k], self.s1.at[k], self.r1.at[k], kv=p)

    def share(self, k, block):
        return remote(self.out.at[block], self.out.at[block], self.s2.at[k], self.r2.at[block], kv=self.peer(k))

    def run(self):
        n, me = self.g.n_kv, self.g.kv
        for k in range(1, n):
            self.part(k).start()
        total = self.sb[me].astype(F32)
        for k in range(1, n):
            self.part(k).wait_recv()
            total = total + self.rb[k].astype(F32)
        self.out[me] = total.astype(self.out.dtype)
        for k in range(1, n):
            self.share(k, me).start()
        for k in range(1, n):
            self.share(k, self.peer(k)).wait_recv()

    def drain(self):
        for k in range(1, self.g.n_kv):
            self.part(k).wait_send()
            self.share(k, self.g.kv).wait_send()


NAMES = (
    "tokens", "norm_gain", "wq", "wk", "wv", "wi", "wf", "bi", "bf", "mem", "nrm", "stab",
    "keys", "vals", "ipre", "fpre", "lens", "hgain", "wo", "mgain", "wg", "wu", "wd",
)
HELD = ("keys", "mem", "vals", "wo", "wg", "wu", "wd")


def kernel(n_tp, n_kv, model, scratch_names, *refs):
    ins = dict(zip(NAMES, refs))
    out = refs[len(NAMES)]
    sc = dict(zip(scratch_names, refs[len(NAMES) + 1:]))
    g = Ring(n_tp, n_kv)
    rows, feats = ins["tokens"].shape
    r, heads, block, size = ins["keys"].shape
    width = heads * size
    every = ins["wi"].shape[1]

    loads = {}
    for i, name in enumerate(HELD):
        loads[name] = pltpu.make_async_copy(ins[name], sc["v_" + name], sc["load_sem"].at[i])
        loads[name].start()

    barrier = pltpu.get_barrier_semaphore()
    for k in range(1, g.nz):
        pl.semaphore_signal(barrier, inc=1, device_id={"tp": g.same(g.up(k))}, device_id_type=MESH)
    pl.semaphore_signal(barrier, inc=1, device_id={"tp": g.partner}, device_id_type=MESH)
    for k in range(1, n_kv):
        pl.semaphore_signal(barrier, inc=1, device_id={"kv": lax.rem(g.kv + k, n_kv)}, device_id_type=MESH)

    def rs(name):
        parts = [sc[f"{name}_{p}"] for p in ("sb", "rb1", "sb2", "rb2")]
        sems = [sc[f"{name}_{p}"] for p in ("s1", "r1", "s2", "r2")]
        return ReduceScatter(g, *parts, sems)

    wide = ins["tokens"][...].astype(F32)
    scaled = (wide * ins["norm_gain"][...]).astype(BF16)
    small_sb = sc["small_sb"]
    small_sb[:, :, 0:every] = dot32(scaled, ins["wi"][...]).reshape(n_tp, r, every)
    small_sb[:, :, every:2 * every] = dot32(scaled, ins["wf"][...]).reshape(n_tp, r, every)
    small_sb[:, :, 2 * every:2 * every + 1] = jnp.sum(wide * wide, axis=1, keepdims=True).reshape(n_tp, r, 1)
    qkv_sb = sc["qkv_sb"]
    for i, name in enumerate(("wq", "wk", "wv")):
        qkv_sb[:, :, i * width:(i + 1) * width] = (
            dot32(scaled, ins[name][...]).astype(BF16).reshape(n_tp, r, width)
        )
    pl.semaphore_wait(barrier, g.nz + n_kv - 1)
    small, qkv = rs("small"), rs("qkv")
    small.start()
    qkv.start()
    small.middle()
    qkv.middle()

    row_of = lax.broadcasted_iota(jnp.int32, (r, block), 0)
    position = lax.broadcasted_iota(jnp.int32, (r, block), 1)
    length = jnp.zeros((r, block), jnp.int32)
    for b in range(r):
        length = jnp.where(row_of == b, ins["lens"][b], length)
    live = position < length
    before = lax.broadcasted_iota(jnp.int32, (block, block), 0)
    after_mask = (before > lax.broadcasted_iota(jnp.int32, (block, block), 1)).astype(F32)
    later, whole_forget, cached_in = [], [], []
    for h in range(heads):
        cached = jnp.where(live, log_sigmoid(ins["fpre"][:, h, :] + ins["bf"][h]), 0.0)
        later.append(
            jnp.dot(cached, after_mask, precision=lax.Precision.HIGHEST, preferred_element_type=F32)
        )
        whole_forget.append(jnp.sum(cached, axis=-1, keepdims=True))
        cached_in.append(ins["ipre"][:, h, :] + ins["bi"][h])

    sums = small.end()
    square = sums[:, 2 * every:2 * every + 1]
    scale = lax.rsqrt(square / model + epsilon)
    lane = lax.broadcasted_iota(jnp.int32, sums.shape, 1)

    def column(at):
        return jnp.sum(jnp.where(lane == at, sums, 0.0), axis=-1, keepdims=True)

    projected = qkv.end() * scale
    query = (projected[:, :width] * size ** (-0.5)).astype(BF16)
    new_key = projected[:, width:2 * width].astype(BF16).astype(F32)
    new_value = projected[:, 2 * width:].astype(BF16).astype(F32)

    loads["keys"].wait()
    loads["mem"].wait()
    q_of = [query[:, h * size:(h + 1) * size] for h in range(heads)]
    row_v = lax.broadcasted_iota(jnp.int32, (r, size), 0)
    group = 4 if r % 4 == 0 else 1

    def scan_keys(i, carry):
        scores, states = list(carry[0]), list(carry[1])
        for j in range(group):
            b = i * group + j
            for h in range(heads):
                s = dot_t(q_of[h], sc["v_keys"][b, h])
                m = dot32(q_of[h], sc["v_mem"][b, h].astype(BF16))
                scores[h] = jnp.where(row_of == b, s, scores[h])
                states[h] = jnp.where(row_v == b, m, states[h])
        return tuple(scores), tuple(states)

    none_s = tuple(jnp.zeros((r, block), F32) for _ in range(heads))
    none_v = tuple(jnp.zeros((r, size), F32) for _ in range(heads))
    scores, states = lax.fori_loop(0, r // group, scan_keys, (none_s, none_v))

    probs, new_weights, state_weights, denominators = [], [], [], []
    for h in range(heads):
        log_in = column(g.kv * heads + h) * scale + ins["bi"][h]
        log_forget = log_sigmoid(column(every + g.kv * heads + h) * scale + ins["bf"][h])
        exponent = jnp.where(live, later[h] + log_forget + cached_in[h], -jnp.inf)
        carried = whole_forget[h] + log_forget + ins["stab"][:, h:h + 1]
        most = jnp.maximum(jnp.maximum(jnp.max(exponent, axis=-1, keepdims=True), carried), log_in)
        weight = jnp.exp(exponent - most) * scores[h]
        q_wide = q_of[h].astype(F32)
        new_w = jnp.exp(log_in - most) * jnp.sum(
            q_wide * new_key[:, h * size:(h + 1) * size], axis=-1, keepdims=True
        )
        state_w = jnp.exp(carried - most)
        norm = jnp.sum(ins["nrm"][:, h, :] * q_wide, axis=-1, keepdims=True)
        denominators.append(jnp.sum(weight, axis=-1, keepdims=True) + new_w + state_w * norm)
        probs.append(weight.astype(BF16))
        new_weights.append(new_w)
        state_weights.append(state_w)

    loads["vals"].wait()

    def scan_values(i, carry):
        sums_v = list(carry)
        for j in range(group):
            b = i * group + j
            for h in range(heads):
                s = dot32(probs[h], sc["v_vals"][b, h])
                sums_v[h] = jnp.where(row_v == b, s, sums_v[h])
        return tuple(sums_v)

    block_sums = lax.fori_loop(0, r // group, scan_values, none_v)
    heads_buf = sc["head_buf"]
    for h in range(heads):
        at = slice(h * size, (h + 1) * size)
        numerator = block_sums[h] + new_weights[h] * new_value[:, at] + state_weights[h] * states[h]
        cell = numerator / jnp.maximum(jnp.abs(denominators[h]), 1.0)
        heads_buf[g.t, :, at] = (cell * ins["hgain"][:, at]).astype(BF16)

    head_gather = Gather(g, heads_buf, [sc[f"head_{p}"] for p in ("s", "f", "r")])
    head_gather.run()

    loads["wo"].wait()
    att = dot32(heads_buf[...].reshape(rows, width), sc["v_wo"][...])
    sc["att_sb"][...] = att.astype(BF16).reshape(n_kv, rows // n_kv, feats)
    att_sum = SumOverKv(
        g, sc["att_sb"], sc["att_rb"], sc["att_out"], [sc[f"att_{p}"] for p in ("s1", "r1", "s2", "r2")]
    )
    att_sum.run()
    residual = ins["tokens"][...].astype(F32) + sc["att_out"][...].reshape(rows, feats).astype(F32)
    sc["res"][...] = residual
    sc["mid"][...] = (residual * ins["mgain"][...]).astype(BF16)
    square = jnp.sum(residual * residual, axis=1, keepdims=True)
    sc["msq_sb"][...] = jnp.broadcast_to(square, (rows, 128)).reshape(n_tp, r, 128)

    msq, gate, up = rs("msq"), rs("gate"), rs("up")
    hidden_dev = ins["wg"].shape[1]
    tile = 256

    def project(weight, target):
        if hidden_dev % tile:
            target[...] = dot32(sc["mid"][...], weight[...]).astype(BF16).reshape(n_tp, r, hidden_dev)
            return

        def step(i, _):
            at = pl.ds(pl.multiple_of(i * tile, tile), tile)
            target[:, :, at] = dot32(sc["mid"][...], weight[:, at]).astype(BF16).reshape(n_tp, r, tile)
            return 0

        lax.fori_loop(0, hidden_dev // tile, step, 0)

    loads["wg"].wait()
    project(sc["v_wg"], sc["gate_sb"])
    gate.start()
    msq.start()
    loads["wu"].wait()
    project(sc["v_wu"], sc["up_sb"])
    gate.middle()
    up.start()
    msq.middle()
    up.middle()
    second = lax.rsqrt(msq.end()[:, 0:1] / model + epsilon)
    gate_pre = gate.end() * second
    silu = gate_pre / (1.0 + jnp.exp(-gate_pre))
    hid = (silu * (up.end() * second)).astype(BF16)
    sc["hid_buf"][g.t] = hid
    hid_gather = Gather(g, sc["hid_buf"], [sc[f"hid_{p}"] for p in ("s", "f", "r")])
    hid_gather.run()
    loads["wd"].wait()
    half = feats // 2 if feats % 256 == 0 else feats
    for at in range(0, feats, half):
        part = dot32(sc["hid_buf"][...].reshape(rows, hidden_dev), sc["v_wd"][:, at:at + half])
        sc["ffn_sb"][:, :, at:at + half] = part.astype(BF16).reshape(n_kv, rows // n_kv, half)
    ffn_sum = SumOverKv(
        g, sc["ffn_sb"], sc["ffn_rb"], sc["ffn_out"], [sc[f"ffn_{p}"] for p in ("s1", "r1", "s2", "r2")]
    )
    ffn_sum.run()
    out[...] = sc["res"][...] + sc["ffn_out"][...].reshape(rows, feats).astype(F32)
    for item in (small, qkv, head_gather, att_sum, msq, gate, up, hid_gather, ffn_sum):
        item.drain()


def body(n_tp, n_kv, *args):
    arrays = dict(zip(NAMES, args))
    rows, feats = arrays["tokens"].shape
    r, heads, block, size = arrays["keys"].shape
    width = heads * size
    hidden_dev = arrays["wg"].shape[1]
    nz = n_tp // 2
    for name in ("norm_gain", "hgain", "mgain"):
        arrays[name] = arrays[name].reshape(1, -1)
    dma = pltpu.SemaphoreType.DMA
    scratch = {"v_" + n: pltpu.VMEM(arrays[n].shape, arrays[n].dtype) for n in HELD}
    scratch["load_sem"] = dma((len(HELD),))
    for name, w, dtype in (
        ("small", 128, F32), ("qkv", 3 * width, BF16), ("msq", 128, F32),
        ("gate", hidden_dev, BF16), ("up", hidden_dev, BF16),
    ):
        scratch[name + "_sb"] = pltpu.VMEM((n_tp, r, w), dtype)
        for p in ("rb1", "sb2", "rb2"):
            scratch[f"{name}_{p}"] = pltpu.VMEM((nz, r, w), dtype)
        for p in ("s1", "r1", "s2", "r2"):
            scratch[f"{name}_{p}"] = dma((nz,))
    for name, w in (("head", width), ("hid", hidden_dev)):
        scratch[name + "_buf"] = pltpu.VMEM((n_tp, r, w), BF16)
        scratch[name + "_s"] = dma((nz,))
        scratch[name + "_f"] = dma((nz,))
        scratch[name + "_r"] = dma((n_tp,))
    for name in ("att", "ffn"):
        for p in ("sb", "rb", "out"):
            scratch[f"{name}_{p}"] = pltpu.VMEM((n_kv, rows // n_kv, feats), BF16)
        for p in ("s1", "r1", "s2", "r2"):
            scratch[f"{name}_{p}"] = dma((n_kv,))
    scratch["res"] = pltpu.VMEM((rows, feats), F32)
    scratch["mid"] = pltpu.VMEM((rows, feats), BF16)

    def spec(name):
        if name in HELD:
            return pl.BlockSpec(memory_space=pl.ANY)
        if name in ("bi", "bf", "lens"):
            return pl.BlockSpec(memory_space=pltpu.SMEM)
        return pl.BlockSpec(memory_space=pltpu.VMEM)

    return pl.pallas_call(
        functools.partial(kernel, n_tp, n_kv, feats * n_tp, tuple(scratch)),
        out_shape=jax.ShapeDtypeStruct((rows, feats), F32),
        in_specs=[spec(n) for n in NAMES],
        out_specs=pl.BlockSpec(memory_space=pltpu.VMEM),
        scratch_shapes=list(scratch.values()),
        compiler_params=pltpu.CompilerParams(
            collective_id=0, has_side_effects=True, vmem_limit_bytes=56 * 1024 * 1024
        ),
    )(*[arrays[n] for n in NAMES])


def solution(mesh):
    placed = (
        P(None, "tp"), P("tp"), P("tp", "kv"), P("tp", "kv"), P("tp", "kv"), P("tp", None), P("tp", None),
        P("kv"), P("kv"), P("tp", "kv", None, None), P("tp", "kv", None), P("tp", "kv"),
        P("tp", "kv", None, None), P("tp", "kv", None, None), P("tp", "kv", None), P("tp", "kv", None),
        P("tp"), P("kv"), P("kv", "tp"), P("tp"), P("tp", "kv"), P("tp", "kv"), P("kv", "tp"),
    )
    run = functools.partial(body, mesh.shape["tp"], mesh.shape["kv"])
    return jax.shard_map(run, mesh=mesh, in_specs=placed, out_specs=P(None, "tp"), check_vma=False)
```

time: 377 us -> 75.8 us (0.20)
  waiting for transfers between devices: 266 us -> 0 us
  Pallas kernels: 0 us -> 68.9 us
  blocking collectives: 48.3 us -> 0 us
  matrix products: 27.9 us -> 0 us
  between operations: 14.5 us -> 0.01 us
  other arithmetic: 8.77 us -> 0 us
  local copies, waits for them, and re-layouts: 10.6 us -> 5.98 us
    psum x3 -> x0, waiting for transfers between devices: 140 us -> none  [the longest x1 56.5 us: body(): gate_sum, up_sum, mid_sum = lax.psum((gate_part, up_part, mid_square), 'tp')]
    reduce_scatter x3 -> x0, waiting for transfers between devices: 90.1 us -> none  [the longest x1 31.1 us: body(): lax.psum_scatter(partial_of(key_weight), 'tp', scatter_dimension=0, tiled...]
    pallas_call x0 -> x1, Pallas kernels: none -> 68.9 us  [body(): pl.pallas_call(functools.partial(kernel, n_tp, n_kv, feats * n_tp, tuple(...]
    unnamed x10 -> x0, waiting for transfers between devices: 35.3 us -> none
    dot_general x11 -> x0, matrix products: 24.4 us -> none  [the longest x3 5.08 us: partial_of(): return jnp.dot(scaled_in, weight, preferred_element_type=jnp.float32)]
    unnamed x1 -> x0, blocking collectives: 18.1 us -> none
    psum x1 -> x0, blocking collectives: 16.2 us -> none  [body(): gate_sum, up_sum, mid_sum = lax.psum((gate_part, up_part, mid_square), 'tp')]
    all_gather x1 -> x0, blocking collectives: 14 us -> none  [body(): lax.all_gather(head_out, 'tp', axis=0, tiled=True)]
  transfers between devices with their start and end apart: 8 -> 0, of which waited for: 8 -> 0; matrix products, arithmetic and copies ran while one was open for 4% -> 0% of each run, Pallas kernels for 0% -> 0%
where the time goes in v1:
time: 75.8 us; the launch traced here: 74.9 us
  Pallas kernels  68.9 us (91%)
  local copies, waits for them, and re-layouts  5.98 us (8%)
    pallas_call x1, Pallas kernels, body(): pl.pallas_call(functools.partial(kernel, n_tp, n_kv, feats * n_tp, tuple(...  68.9 us
    unnamed x4, local copies, waits for them, and re-layouts  5.98 us

profile of v1, /device:TPU:0, one launch (start us, length us, event | category | flops | bytes accessed | tf_op | source)
XLA Modules:
  0.0 74.9 jit_solution(8221281308869630957)
XLA Ops:
  0.0 1.4 %copy.26.refs_11_ = f32[16,4]{1,0:T(8,128)} copy(f32[16,4]{0,1:T(4,128)} %param.34) | data formatting | bytes 512 | tf_op args[11]
  1.4 1.5 %copy.24.refs_5_ = bf16[512,16]{1,0:T(8,128)(2,1)} copy(bf16[512,16]{0,1:T(8,128)(2,1)} %param.28) | data formatting | bytes 32768 | tf_op args[5]
  2.8 1.5 %copy.25.refs_6_ = bf16[512,16]{1,0:T(8,128)(2,1)} copy(bf16[512,16]{0,1:T(8,128)(2,1)} %param.29) | data formatting | bytes 32768 | tf_op args[6]
  4.3 68.9 %shard_map.217 = f32[128,512]{1,0:T(8,128)} custom-call(bf16[128,512]{1,0:T(8,128)(2,1)} %refs_0_.1, f32[1,512]{1,0:T(1,128)} %bitcast.3, bf16[512,512]{1,0:T(8,128)(2,1)} %refs_2_.1, bf16[512,512]{1,0:T(8,128)(2,1)} %refs_3_.1, bf16[512,512]{1,0:T(8,128)(2,1)} %refs_4_.1, bf16[512,16]{1,0:T(8,128)(2,1)} %copy.24.refs_5_, bf16[512,16]{1,0:T(8,128)(2,1)} %copy.25.refs_6_, ...), custom_call_target="tpu_custom_call" | custom-call | tf_op jit(solution)/shard_map/pallas_call | solution.py:415
  73.3 1.7 %copy.28 = f32[128,512]{1,0:T(8,128)} copy(f32[128,512]{1,0:T(8,128)} %shard_map.217) | data formatting | bytes 524288
